TPU v7x, 512 devices: a whole 4x4x16 slice. The times are simulated.
512 devices in a mesh: sp: 64 (over z, y), tp: 8 (over x, core).
Axes of the slice: x: 4, y: 4, z: 16, core: 2. Of those that a mesh axis runs over, the one named last changes fastest.
Arguments:
- residual: bfloat16 [8192, 2048], P(('sp', 'tp')), may hold values from -24 to 24
- query_small: bfloat16 [8192, 768], P('sp', 'tp'), may hold values from -64 to 64
- query_large: bfloat16 [8192, 1280], P('sp', 'tp'), may hold values from -64 to 64
- latent: bfloat16 [8192, 256], P('sp'), may hold values from -6 to 6
- rope_key: bfloat16 [8192, 32], P('sp'), may hold values from -48 to 48
- key_up_small: bfloat16 [256, 512], P(None, 'tp'), may hold values from -0.375 to 0.375
- value_up_small: bfloat16 [256, 512], P(None, 'tp'), may hold values from -0.375 to 0.375
- key_up_large: bfloat16 [256, 1024], P(None, 'tp'), may hold values from -0.375 to 0.375
- value_up_large: bfloat16 [256, 1024], P(None, 'tp'), may hold values from -0.375 to 0.375
- out_small: bfloat16 [512, 2048], P('tp'), may hold values from -0.625 to 0.625
- out_large: bfloat16 [1024, 2048], P('tp'), may hold values from -0.625 to 0.625
- norm_gain: bfloat16 [2048], replicated, may hold values from 0.099609375 to 1.8984375
- gate_weight: bfloat16 [2048, 5632], P('sp', 'tp'), may hold values from -0.125 to 0.125
- up_weight: bfloat16 [2048, 5632], P('sp', 'tp'), may hold values from -0.125 to 0.125
- down_weight: bfloat16 [2048, 5632], P('sp', 'tp'), may hold values from -0.21875 to 0.21875
Outputs:
- layer_out: bfloat16 [8192, 2048], P(('sp', 'tp'))
All inputs are finite; a program needn't handle non-finite values.
Results may differ from a plain program's by a relative error of at most 0.017.
Values may be sent and summed in bfloat16 or wider, within the bound.
No kernel may reach another device: no remote copies, remote signals or barrier semaphores. Data moves between devices by JAX's collectives and lax.ppermute only.
A program may use at most 64 MiB of HBM per device.

v0:
```python
import jax
import jax.numpy as jnp
from jax import lax
from jax.sharding import PartitionSpec as P

HEAD_SMALL = 64
HEAD_LARGE = 128
ROPE = 32
big_negative = -1e30
rope_base = 500000.0
norm_eps = 1e-06


def cut_along(shard, dim, count):
    before, after = (shard.shape[:dim], shard.shape[dim + 1 :])
    return jnp.moveaxis(shard.reshape(*before, count, -1, *after), dim, 0)


def sent_and_summed(shard, axis, dim):
    count = lax.axis_size(axis)
    tiles = lax.all_to_all(cut_along(shard, dim, count), axis, 0, 0, tiled=True)
    return jnp.sum(tiles.astype(jnp.float32), axis=0)


def sent_together(arrays, axis, dim, along):
    widths = [a.shape[along] for a in arrays]
    both = jnp.concatenate(arrays, axis=along)
    whole = lax.all_gather(both, axis, axis=dim, tiled=True)
    return tuple(jnp.split(whole, [sum(widths[:k]) for k in range(1, len(widths))], axis=along))


def laid_out(tiles, dim):
    lengths = list(tiles.shape[1:])
    lengths[dim] *= tiles.shape[0]
    return jnp.moveaxis(tiles, 0, dim).reshape(lengths)


def from_everyone(shard, axis):
    copies = jnp.broadcast_to(shard, (lax.axis_size(axis), *shard.shape))
    return lax.all_to_all(copies, axis, split_axis=0, concat_axis=0, tiled=True)


def collect(shard, axis, dim):
    return laid_out(from_everyone(shard, axis), dim)


def rotate(vectors, positions):
    span_width = vectors.shape[-1]
    half_width = span_width // 2
    inverse = 1.0 / rope_base ** (jnp.arange(0, span_width, 2, dtype=jnp.float32) / span_width)
    angles = positions.astype(jnp.float32)[:, None] * inverse[None, :]
    angle_shape = (vectors.shape[0],) + (1,) * (vectors.ndim - 2) + (half_width,)
    cosine = jnp.cos(angles).reshape(angle_shape)
    sine_table = jnp.sin(angles).reshape(angle_shape)
    leading = vectors[..., :half_width].astype(jnp.float32)
    trailing = vectors[..., half_width:].astype(jnp.float32)
    turned = jnp.concatenate(
        [leading * cosine - trailing * sine_table, trailing * cosine + leading * sine_table],
        axis=-1,
    )
    return turned.astype(jnp.bfloat16)


def group_update(
    running, nope_part, turned_query, key_rows, value_rows, turned_key, visible, head_size
):
    maxima, totals, summed = running
    head_count = nope_part.shape[0]
    key_count = key_rows.shape[0]
    key_rows = key_rows.reshape(key_count, head_count, head_size)
    value_rows = value_rows.reshape(key_count, head_count, head_size)
    scores = jnp.einsum("hqe,khe->hqk", nope_part, key_rows, preferred_element_type=jnp.float32)
    scores = scores + jnp.einsum(
        "hqr,kr->hqk", turned_query, turned_key, preferred_element_type=jnp.float32
    )
    scores = scores * (head_size + ROPE) ** (-0.5)
    masked = jnp.where(visible[None, :, :], scores, big_negative)
    new_maxima = jnp.maximum(maxima, jnp.max(masked, axis=2))
    weights = jnp.where(visible[None, :, :], jnp.exp(masked - new_maxima[:, :, None]), 0.0)
    totals = jnp.sum(weights, axis=2)
    summed = jnp.einsum(
        "hqk,khe->hqe", weights.astype(jnp.bfloat16), value_rows, preferred_element_type=jnp.float32
    )
    return (new_maxima, totals, summed)


def finish(running):
    maxima, totals, summed = running
    head_count, row_count, head_size = summed.shape
    result = summed / totals[:, :, None]
    return (
        jnp.transpose(result, (1, 0, 2))
        .reshape(row_count, head_count * head_size)
        .astype(jnp.bfloat16)
    )


def shards(
    residual,
    query_small,
    query_large,
    latent,
    rope_key,
    key_up_small,
    value_up_small,
    key_up_large,
    value_up_large,
    out_small,
    out_large,
    norm_gain,
    gate_weight,
    up_weight,
    down_weight,
):
    row_count = query_small.shape[0]
    first_row = lax.axis_index("sp") * row_count
    query_pos = first_row + jnp.arange(row_count, dtype=jnp.int32)
    heads_small = key_up_small.shape[1] // HEAD_SMALL
    heads_large = key_up_large.shape[1] // HEAD_LARGE

    def split_query(query, head_count, head_size):
        shaped = query.reshape(row_count, head_count, head_size + ROPE)
        nope_part = jnp.transpose(shaped[..., :head_size], (1, 0, 2))
        turned = jnp.transpose(rotate(shaped[..., head_size:], query_pos), (1, 0, 2))
        return (nope_part, turned)

    nope_small, turned_small = split_query(query_small, heads_small, HEAD_SMALL)
    nope_large, turned_large = split_query(query_large, heads_large, HEAD_LARGE)

    def initial(head_count, head_size):
        return (
            jnp.full((head_count, row_count), big_negative, jnp.float32),
            jnp.zeros((head_count, row_count), jnp.float32),
            jnp.zeros((head_count, row_count, head_size), jnp.float32),
        )

    starting = (initial(heads_small, HEAD_SMALL), initial(heads_large, HEAD_LARGE))
    part_latent = lax.all_gather(latent, "sp", axis=0, tiled=True)
    part_rope = lax.all_gather(rope_key, "sp", axis=0, tiled=True)
    key_count = part_latent.shape[0]
    key_pos = jnp.arange(key_count, dtype=jnp.int32)

    def compute(running):
        turned_key = rotate(part_rope, key_pos)
        visible = key_pos[None, :] <= query_pos[:, None]
        key_small = jnp.dot(part_latent, key_up_small, preferred_element_type=jnp.float32).astype(
            jnp.bfloat16
        )
        value_small = jnp.dot(
            part_latent, value_up_small, preferred_element_type=jnp.float32
        ).astype(jnp.bfloat16)
        key_large = jnp.dot(part_latent, key_up_large, preferred_element_type=jnp.float32).astype(
            jnp.bfloat16
        )
        value_large = jnp.dot(
            part_latent, value_up_large, preferred_element_type=jnp.float32
        ).astype(jnp.bfloat16)
        small_state = group_update(
            running[0],
            nope_small,
            turned_small,
            key_small,
            value_small,
            turned_key,
            visible,
            HEAD_SMALL,
        )
        large_state = group_update(
            running[1],
            nope_large,
            turned_large,
            key_large,
            value_large,
            turned_key,
            visible,
            HEAD_LARGE,
        )
        return (small_state, large_state)

    def keep(running):
        return running

    running = lax.cond(jnp.int32(0) <= query_pos[-1], compute, keep, starting)
    attended_small = finish(running[0])
    attended_large = finish(running[1])
    mixed = sent_and_summed(
        (
            jnp.dot(attended_small, out_small, preferred_element_type=jnp.float32)
            + jnp.dot(attended_large, out_large, preferred_element_type=jnp.float32)
        ).astype(jnp.bfloat16),
        "tp",
        0,
    ).astype(jnp.bfloat16)
    stream = (residual.astype(jnp.float32) + mixed.astype(jnp.float32)).astype(jnp.bfloat16)
    as_float = stream.astype(jnp.float32)
    normed = as_float * lax.rsqrt(jnp.mean(as_float * as_float, axis=-1, keepdims=True) + norm_eps)
    normed = (normed * norm_gain.astype(jnp.float32)[None, :]).astype(jnp.bfloat16)
    gate_full, up_full, down_full = sent_together((gate_weight, up_weight, down_weight), "sp", 0, 1)
    piece = collect(normed, "tp", 0)
    gate_part = jnp.dot(piece, gate_full, preferred_element_type=jnp.float32)
    up_part = jnp.dot(piece, up_full, preferred_element_type=jnp.float32)
    hidden = (jax.nn.silu(gate_part) * up_part).astype(jnp.bfloat16)
    channel = sent_and_summed(
        lax.dot_general(
            hidden, down_full, (((1,), (1,)), ((), ())), preferred_element_type=jnp.float32
        ).astype(jnp.bfloat16),
        "tp",
        0,
    ).astype(jnp.bfloat16)
    return (as_float + 0.5 * channel.astype(jnp.float32)).astype(jnp.bfloat16)


def solution(mesh):
    placed = (
        P(("sp", "tp"), None),
        P("sp", "tp"),
        P("sp", "tp"),
        P("sp", None),
        P("sp", None),
        P(None, "tp"),
        P(None, "tp"),
        P(None, "tp"),
        P(None, "tp"),
        P("tp", None),
        P("tp", None),
        P(),
        P("sp", "tp"),
        P("sp", "tp"),
        P("sp", "tp"),
    )
    return jax.shard_map(
        shards, mesh=mesh, in_specs=placed, out_specs=P(("sp", "tp"), None), check_vma=False
    )
```

profile of v0, /device:TPU:1, one launch (start us, length us, event | category | flops | bytes accessed | tf_op | source)
XLA Modules:
  0.0 348.7 jit_solution(13543055869742643674)
XLA Ops:
  6.5 0.7 all-gather.3.cloned.1.call-update
  7.3 1.6 concatenate.47
  8.9 0.6 slice.35
  10.2 0.9 fusion.87
  11.1 86.3 %all_gather.10 = bf16[8192,32]{0,1:T(8,128)(2,1)S(1)} all-gather(bf16[128,32]{0,1:T(8,128)(2,1)} %param.21), channel_id=1, replica_groups=mesh['sp'=64,'tp'=8] {'sp'}, dimensions={0}, use_global_device_ids=true | all-gather | bytes 532480 | tf_op jit(solution)/shard_map/all_gather | solution.py:139
  97.3 54.7 %all-gather.3.cloned.1.call-done = bf16[8192,256]{1,0:T(8,128)(2,1)} async-done(((bf16[128,256]{1,0:T(8,128)(2,1)}), bf16[8192,256]{1,0:T(8,128)(2,1)}) %all-gather.3.cloned.1.call-update) | async-done | bytes 4194320 | tf_op jit(solution)/shard_map/all_gather | solution.py:138
  152.0 49.8 %conditional.1 = (f32[1,128]{1,0:T(1,128)S(1)}, f32[1,128,64]{1,2,0:T(8,128)S(1)}, f32[1,128]{1,0:T(1,128)S(1)}, f32[1,128,128]{2,1,0:T(8,128)S(1)}) conditional(s32[]{:T(128)} %bitcast.10, () %tuple.13, (s32[8192]{0:T(1024)S(1)}, s32[128]{0:T(128)S(1)}, bf16[8192,256]{1,0:T(8,128)(2,1)}, bf16[256,64]{0,1:T(8,128)(2,1)}, ...), branch_computations={%region_0.0_spmd, %region_1.6_spmd} | conditional | flops 2583461632 | bytes 62645008 | solution.py:183
  152.0 6.2 %fusion.20 = f32[8192,128]{1,0:T(8,128)} fusion(bf16[8192,256]{1,0:T(8,128)(2,1)} %get-tuple-element.39, bf16[256,64]{0,1:T(8,128)(2,1)} %get-tuple-element.104, bf16[128,1,96]{0,2,1:T(8,128)(2,1)} %get-tuple-element.41), kind=kOutput, calls=%fused_computation.26 | convolution fusion | flops 403177472 | bytes 8437760 | tf_op jit(solution)/shard_map/cond/branch_1_fun/hqe,khe->hqk/dot_general | solution.py:72
  158.3 7.2 %fusion.28 = (bf16[8192,16]{0,1:T(8,128)(2,1)S(1)}, bf16[8192,16]{0,1:T(8,128)(2,1)S(1)}) fusion(f32[8192]{0:T(1024)S(1)} %convert_element_type.101, f32[16]{0:T(128)S(1)} %negate_power_fusion, f32[8192]{0:T(1024)S(1)} %convert_element_type.99, bf16[8192,32]{0,1:T(8,128)(2,1)S(1)} %get-tuple-element.42, f32[8192]{0:T(1024)S(1)} %convert_element_type.103, ...), kind=kLoop, calls=%fused_computation.34 | loop fusion | flops 1835008 | bytes 1179712 | tf_op jit(solution)/shard_map/convert.2
  165.5 5.8 %fusion.93 = (f32[128]{0:T(128)S(1)}, f32[128,8192]{0,1:T(8,128)}) fusion(f32[8192,128]{1,0:T(8,128)} %fusion.20, bf16[1,128,32]{1,2,0:T(8,128)(2,1)S(1)} %get-tuple-element.111, bf16[8192,16]{0,1:T(8,128)(2,1)S(1)} %get-tuple-element.120, bf16[8192,16]{0,1:T(8,128)(2,1)S(1)} %get-tuple-element.119, s32[128]{0:T(128)S(1)} %get-tuple-element.38, ...), kind=kOutput, calls=%fused_computation.110 | convolution fusion | flops 73400192 | bytes 8954880 | tf_op jit(solution)/shard_map/cond/branch_1_fun/hqr,kr->hqk/dot_general | solution.py:73
  171.4 6.3 %fusion.19 = f32[8192,128]{1,0:T(8,128)} fusion(bf16[8192,256]{1,0:T(8,128)(2,1)} %get-tuple-element.39, bf16[256,128]{1,0:T(8,128)(2,1)S(1)} %copy-done.3, bf16[128,1,160]{2,0,1:T(8,128)(2,1)S(1)} %copy.38), kind=kOutput, calls=%fused_computation.25 | convolution fusion | flops 806354944 | bytes 8486912 | tf_op jit(solution)/shard_map/cond/branch_1_fun/hqe,khe->hqk/dot_general | solution.py:72
  177.7 5.8 %fusion.92 = (f32[128]{0:T(128)S(1)}, f32[128,8192]{0,1:T(8,128)}) fusion(f32[8192,128]{1,0:T(8,128)} %fusion.19, bf16[1,128,32]{1,2,0:T(8,128)(2,1)S(1)} %get-tuple-element.115, bf16[8192,16]{0,1:T(8,128)(2,1)S(1)} %get-tuple-element.120, bf16[8192,16]{0,1:T(8,128)(2,1)S(1)} %get-tuple-element.119, s32[128]{0:T(128)S(1)} %get-tuple-element.38, ...), kind=kOutput, calls=%fused_computation.109 | convolution fusion | flops 73400192 | bytes 8954880 | tf_op jit(solution)/shard_map/cond/branch_1_fun/hqr,kr->hqk/dot_general | solution.py:73
  183.5 6.0 %fusion.21 = f32[1,128,128]{2,1,0:T(8,128)S(1)} fusion(bf16[8192,256]{1,0:T(8,128)(2,1)} %get-tuple-element.39, bf16[256,128]{1,0:T(8,128)(2,1)S(1)} %copy-done.6, f32[128,8192]{0,1:T(8,128)} %get-tuple-element.122, f32[128]{0:T(128)S(1)} %get-tuple-element.125, s32[128]{0:T(128)S(1)} %get-tuple-element.38, s32[8192]{0:T(1024)S(1)} %get-tuple-element.46), kind=kOutput, calls=%fused_computation.27 | convolution fusion | flops 810549248 | bytes 8553472 | tf_op jit(solution)/shard_map/cond/branch_1_fun/hqk,khe->hqe/dot_general | solution.py:81
  189.5 5.7 %fusion.24 = f32[1,128,64]{1,2,0:T(8,128)S(1)} fusion(f32[128,8192]{0,1:T(8,128)} %get-tuple-element.124, f32[128]{0:T(128)S(1)} %get-tuple-element.126, s32[128]{0:T(128)S(1)} %get-tuple-element.38, s32[8192]{0:T(1024)S(1)} %get-tuple-element.46, bf16[8192,256]{1,0:T(8,128)(2,1)} %get-tuple-element.39, bf16[256,64]{0,1:T(8,128)(2,1)S(1)} %copy-done.7), kind=kOutput, calls=%fused_computation.28 | convolution fusion | flops 407371776 | bytes 8487936 | tf_op jit(solution)/shard_map/cond/branch_1_fun/hqk,khe->hqe/dot_general | solution.py:81
  195.2 6.6 %fusion.9 = (f32[128]{0:T(128)S(1)}, f32[128]{0:T(128)S(1)}) fusion(f32[128,8192]{0,1:T(8,128)} %get-tuple-element.122, f32[128]{0:T(128)S(1)} %get-tuple-element.125, s32[128]{0:T(128)S(1)} %get-tuple-element.38, s32[8192]{0:T(1024)S(1)} %get-tuple-element.46, f32[128,8192]{0,1:T(8,128)} %get-tuple-element.124, f32[128]{0:T(128)S(1)} %get-tuple-element.126), kind=kLoop, calls=%fused_computation.17 | loop fusion | flops 7339776 | bytes 8423936 | tf_op jit(solution)/shard_map/cond/branch_1_fun/reduce_sum | solution.py:80
  202.2 1.2 fusion.45
  203.3 14.8 %all-to-all-start = ((bf16[8,16,2048]{2,1,0:T(8,128)(2,1)}), bf16[8,16,2048]{2,1,0:T(8,128)(2,1)S(1)}, u32[]{:S(2)}, u32[]{:S(2)}) async-start(bf16[8,16,2048]{2,1,0:T(8,128)(2,1)} %bitcast.21), calls=%async_computation | async-start | bytes 1048576 | tf_op jit(solution)/shard_map/all_to_all | solution.py:21
  218.1 9.3 %all-to-all-done = bf16[8,16,2048]{2,1,0:T(8,128)(2,1)S(1)} async-done(((bf16[8,16,2048]{2,1,0:T(8,128)(2,1)}), bf16[8,16,2048]{2,1,0:T(8,128)(2,1)S(1)}, u32[]{:S(2)}, u32[]{:S(2)}) %all-to-all-start) | async-done | bytes 524320 | tf_op jit(solution)/shard_map/all_to_all | solution.py:21
  227.8 12.9 %all_to_all.15 = bf16[8,16,2048]{2,1,0:T(8,128)(2,1)S(1)} all-to-all(bf16[8,16,2048]{2,1,0:T(8,128)(2,1)S(1)} %broadcast_in_dim.17), channel_id=1, replica_groups=mesh['sp'=64,'tp'=8] {'tp'}, dimensions={0} | all-to-all | bytes 1048576 | tf_op jit(solution)/shard_map/all_to_all | solution.py:40
  240.7 68.3 %all-gather.5.cloned.1.call-done = bf16[2048,2112]{1,0:T(8,128)(2,1)} async-done(((bf16[32,2112]{1,0:T(8,128)(2,1)}), bf16[2048,2112]{1,0:T(8,128)(2,1)}) %all-gather.5.cloned.1.call-update) | async-done | bytes 8650768 | tf_op jit(solution)/shard_map/all_gather | solution.py:28
  309.0 3.2 fusion.43
  312.2 7.2 %fusion.46 = bf16[128,2048]{1,0:T(8,128)(2,1)S(1)} fusion(bf16[2048,2112]{1,0:T(8,128)(2,1)} %all-gather.5.cloned.1.call-done, bf16[128,2048]{1,0:T(8,128)(2,1)S(1)} %bitcast.67, f32[128,704]{0,1:T(8,128)S(1)} %fusion.43), kind=kOutput, calls=%fused_computation.58 | convolution fusion | flops 739000320 | bytes 7700480 | tf_op jit(solution)/shard_map/dot_general | solution.py:204
  319.5 21.6 %all_to_all.16 = bf16[8,16,2048]{2,1,0:T(8,128)(2,1)S(1)} all-to-all(bf16[8,16,2048]{2,1,0:T(8,128)(2,1)S(1)} %bitcast.68), channel_id=1, replica_groups=mesh['sp'=64,'tp'=8] {'tp'}, dimensions={0} | all-to-all | bytes 1048576 | tf_op jit(solution)/shard_map/all_to_all | solution.py:21
  341.2 0.7 fusion.66
  (39 shorter events, 1.0 us)
Async XLA Ops:
  6.5 195.6 %copy-start = (bf16[128,2048]{1,0:T(8,128)(2,1)S(1)}, bf16[128,2048]{1,0:T(8,128)(2,1)}, u32[]{:S(2)}) copy-start(bf16[128,2048]{1,0:T(8,128)(2,1)} %param.27) | copy-start | bytes 1572868
  6.5 145.5 %all-gather.3.cloned.1.call-start = ((), (), s32[]{:S(2)}) async-start(), calls=%async_computation.3 | async-start | bytes 4259840 | tf_op jit(solution)/shard_map/all_gather | solution.py:138
  7.3 301.8 %all-gather.5.cloned.1.call-start = ((), (), s32[]{:S(2)}) async-start(), calls=%async_computation.4 | async-start | bytes 9052160 | tf_op jit(solution)/shard_map/all_gather | solution.py:28
  152.0 49.8 %copy-start.2 = (bf16[64,2048]{1,0:T(8,128)(2,1)S(1)}, bf16[64,2048]{1,0:T(8,128)(2,1)}, u32[]{:S(2)}) copy-start(bf16[64,2048]{1,0:T(8,128)(2,1)} %param.26) | copy-start | bytes 786436
  165.4 5.8 %copy-start.4 = (bf16[128,1,160]{0,2,1:T(8,128)(2,1)S(1)}, bf16[128,1,160]{0,2,1:T(8,128)(2,1)}, u32[]{:S(2)}) copy-start(bf16[128,1,160]{0,2,1:T(8,128)(2,1)} %get-tuple-element.114) | copy-start | bytes 122884 | tf_op jit(solution)/shard_map/cond
  165.5 5.9 %copy-start.3 = (bf16[256,128]{1,0:T(8,128)(2,1)S(1)}, bf16[256,128]{1,0:T(8,128)(2,1)}, u32[]{:S(2)}) copy-start(bf16[256,128]{1,0:T(8,128)(2,1)} %get-tuple-element.67) | copy-start | bytes 196612 | tf_op jit(solution)/shard_map/cond
  177.7 5.8 %copy-start.6 = (bf16[256,128]{1,0:T(8,128)(2,1)S(1)}, bf16[256,128]{1,0:T(8,128)(2,1)}, u32[]{:S(2)}) copy-start(bf16[256,128]{1,0:T(8,128)(2,1)} %get-tuple-element.68) | copy-start | bytes 196612 | tf_op jit(solution)/shard_map/cond
  183.5 6.0 %copy-start.7 = (bf16[256,64]{0,1:T(8,128)(2,1)S(1)}, bf16[256,64]{0,1:T(8,128)(2,1)}, u32[]{:S(2)}) copy-start(bf16[256,64]{0,1:T(8,128)(2,1)} %get-tuple-element.112) | copy-start | bytes 98308 | tf_op jit(solution)/shard_map/cond
  201.8 16.3 %copy-start.5 = (bf16[2048]{0:T(1024)(128)(2,1)S(1)}, bf16[2048]{0:T(1024)(128)(2,1)}, u32[]{:S(2)}) copy-start(bf16[2048]{0:T(1024)(128)(2,1)} %param.28) | copy-start | bytes 12292
  201.8 25.7 %copy-start.1 = (bf16[16,2048]{1,0:T(8,128)(2,1)S(1)}, bf16[16,2048]{1,0:T(8,128)(2,1)}, u32[]{:S(2)}) copy-start(bf16[16,2048]{1,0:T(8,128)(2,1)} %param.17) | copy-start | bytes 196612
  203.3 24.1 %all-to-all-start = ((bf16[8,16,2048]{2,1,0:T(8,128)(2,1)}), bf16[8,16,2048]{2,1,0:T(8,128)(2,1)S(1)}, u32[]{:S(2)}, u32[]{:S(2)}) async-start(bf16[8,16,2048]{2,1,0:T(8,128)(2,1)} %bitcast.21), calls=%async_computation | async-start | bytes 1048576 | tf_op jit(solution)/shard_map/all_to_all | solution.py:21
Sparse Core Ops, SparseCore 0:
  10.3 141.7 all-gather.2
  155.0 154.0 all-gather.4
where the time goes:
time: 349 us
  waiting for transfers between devices  133 us (38%)
  blocking collectives  121 us (35%)
  matrix products  47.6 us (14%)
  other arithmetic  15.8 us (5%)
  starting transfers between devices  14.8 us (4%)
  between operations  14.2 us (4%)
    all_gather x1, blocking collectives, shards(): part_rope = lax.all_gather(rope_key, 'sp', axis=0, tiled=True)  86.3 us
    all_gather x1, waiting for transfers between devices, sent_together(): whole = lax.all_gather(both, axis, axis=dim, tiled=True)  68.3 us
    all_gather x1, waiting for transfers between devices, shards(): part_latent = lax.all_gather(latent, 'sp', axis=0, tiled=True)  54.7 us
    all_to_all x1, blocking collectives, sent_and_summed(): tiles = lax.all_to_all(cut_along(shard, dim, count), axis, 0, 0, tiled=True)  21.6 us
    all_to_all x1, starting transfers between devices, sent_and_summed(): tiles = lax.all_to_all(cut_along(shard, dim, count), axis, 0, 0, tiled=True)  14.8 us
    all_to_all x1, blocking collectives, from_everyone(): return lax.all_to_all(copies, axis, split_axis=0, concat_axis=0, tiled=True)  12.9 us
    dot_general x2, matrix products, group_update(): jnp.einsum('hqe,khe->hqk', nope_part, key_rows, preferred_element_type=jn...  12.5 us
    dot_general x2, matrix products, group_update(): jnp.einsum('hqk,khe->hqe', weights.astype(jnp.bfloat16), value_rows, pref...  11.7 us
  transfers between devices with their start and end apart: 3, of which 3 were waited for; matrix products, arithmetic and copies ran while one was open for 16% of the time, Pallas kernels for 0%

commit v1 on v0

--- a/solution.py
+++ b/solution.py
@@ -135,7 +135,9 @@
         )
 
     starting = (initial(heads_small, HEAD_SMALL), initial(heads_large, HEAD_LARGE))
-    part_latent = lax.all_gather(latent, "sp", axis=0, tiled=True)
+    part_latent = jnp.concatenate(
+        lax.all_to_all(jnp.stack([latent] * lax.axis_size("sp")), "sp", 0, 0), axis=0
+    )
     part_rope = lax.all_gather(rope_key, "sp", axis=0, tiled=True)
     key_count = part_latent.shape[0]
     key_pos = jnp.arange(key_count, dtype=jnp.int32)

time: 349 us -> 448 us (1.28)
  blocking collectives: 121 us -> 295 us
  waiting for transfers between devices: 133 us -> 18.7 us
  starting transfers between devices: 14.8 us -> 50.6 us
    all_gather x1, blocking collectives: 86.3 us -> 282 us  [shards(): part_rope = lax.all_gather(rope_key, 'sp', axis=0, tiled=True)]
    all_gather x1, waiting for transfers between devices: 68.3 us -> 0.01 us  [sent_together(): whole = lax.all_gather(both, axis, axis=dim, tiled=True)]
    all_gather x1 -> x0, waiting for transfers between devices: 54.7 us -> none  [shards(): part_latent = lax.all_gather(latent, 'sp', axis=0, tiled=True)]
    all_to_all x0 -> x2, starting transfers between devices: none -> 24 us  [the longest x1 19.7 us: shards(): lax.all_to_all(jnp.stack([latent] * lax.axis_size('sp')), 'sp', 0, 0)]
    all_to_all x1 -> x0, blocking collectives: 12.9 us -> none  [from_everyone(): return lax.all_to_all(copies, axis, split_axis=0, concat_axis=0, tiled=True)]
    all_to_all x1, starting transfers between devices: 14.8 us -> 26.6 us  [sent_and_summed(): tiles = lax.all_to_all(cut_along(shard, dim, count), axis, 0, 0, tiled=True)]
    all_to_all x0 -> x2, waiting for transfers between devices: none -> 9.38 us  [the longest x1 9.38 us: from_everyone(): return lax.all_to_all(copies, axis, split_axis=0, concat_axis=0, tiled=True)]
    all_to_all x1, blocking collectives: 21.6 us -> 12.7 us  [sent_and_summed(): tiles = lax.all_to_all(cut_along(shard, dim, count), axis, 0, 0, tiled=True)]
  transfers between devices with their start and end apart: 3 -> 4, of which waited for: 3 -> 2; matrix products, arithmetic and copies ran while one was open for 16% -> 12% of each run, Pallas kernels for 0% -> 0%
where the time goes in v1:
time: 448 us; the launch traced here: 447 us
  blocking collectives  295 us (66%)
  starting transfers between devices  50.6 us (11%)
  matrix products  47.5 us (11%)
  waiting for transfers between devices  18.7 us (4%)
  other arithmetic  15 us (3%)
  between operations  14.3 us (3%)
  local copies, waits for them, and re-layouts  5.73 us (1%)
    all_gather x1, blocking collectives, shards(): part_rope = lax.all_gather(rope_key, 'sp', axis=0, tiled=True)  282 us
    all_to_all x1, starting transfers between devices, sent_and_summed(): tiles = lax.all_to_all(cut_along(shard, dim, count), axis, 0, 0, tiled=True)  26.6 us
    all_to_all x1, starting transfers between devices, shards(): lax.all_to_all(jnp.stack([latent] * lax.axis_size('sp')), 'sp', 0, 0)  19.7 us
    all_to_all x1, blocking collectives, sent_and_summed(): tiles = lax.all_to_all(cut_along(shard, dim, count), axis, 0, 0, tiled=True)  12.7 us
    dot_general x2, matrix products, group_update(): jnp.einsum('hqe,khe->hqk', nope_part, key_rows, preferred_element_type=jn...  12.5 us
    dot_general x2, matrix products, group_update(): jnp.einsum('hqk,khe->hqe', weights.astype(jnp.bfloat16), value_rows, pref...  11.6 us
    dot_general x2, matrix products, group_update(): jnp.einsum('hqr,kr->hqk', turned_query, turned_key, preferred_element_typ...  11.5 us
    all_to_all x1, waiting for transfers between devices, from_everyone(): return lax.all_to_all(copies, axis, split_axis=0, concat_axis=0, tiled=True)  9.38 us
  transfers between devices with their start and end apart: 4, of which 2 were waited for; matrix products, arithmetic and copies ran while one was open for 12% of the time, Pallas kernels for 0%

profile of v1, /device:TPU:1, one launch (start us, length us, event | category | flops | bytes accessed | tf_op | source)
XLA Modules:
  0.0 446.9 jit_solution(10610583475535515243)
XLA Ops:
  6.5 3.3 stack.2
  9.9 19.7 %all-to-all-start = ((bf16[64,128,256]{2,1,0:T(8,128)(2,1)}), bf16[64,128,256]{2,1,0:T(8,128)(2,1)}, u32[]{:S(2)}, u32[]{:S(2)}) async-start(bf16[64,128,256]{2,1,0:T(8,128)(2,1)} %stack.2), calls=%async_computation | async-start | bytes 8388608 | tf_op jit(solution)/shard_map/all_to_all | solution.py:139
  29.7 0.8 concatenate.47
  30.5 0.6 slice.35
  31.9 282.0 %all_gather.6 = bf16[8192,32]{0,1:T(8,128)(2,1)S(1)} all-gather(bf16[128,32]{0,1:T(8,128)(2,1)S(1)} %copy-done.10), channel_id=1, replica_groups=mesh['sp'=64,'tp'=8] {'sp'}, dimensions={0}, use_global_device_ids=true | all-gather | bytes 532480 | tf_op jit(solution)/shard_map/all_gather | solution.py:141
  314.0 49.8 %conditional.1 = (f32[1,128]{1,0:T(1,128)S(1)}, f32[1,128,64]{1,2,0:T(8,128)S(1)}, f32[1,128]{1,0:T(1,128)S(1)}, f32[1,128,128]{2,1,0:T(8,128)S(1)}) conditional(s32[]{:T(128)} %bitcast.11, () %tuple.13, (s32[8192]{0:T(1024)S(1)}, s32[128]{0:T(128)S(1)}, bf16[64,128,256]{2,1,0:T(8,128)(2,1)}, bf16[256,64]{0,1:T(8,128)(2,1)S(1)}, ...), branch_computations={%region_0.0_spmd, %region_1.6_spmd} | conditional | flops 2583461632 | bytes 61825696 | solution.py:185
  314.2 6.2 %fusion.20 = f32[8192,128]{1,0:T(8,128)} fusion(bf16[8192,256]{1,0:T(8,128)(2,1)} %bitcast, bf16[256,64]{0,1:T(8,128)(2,1)S(1)} %get-tuple-element.105, bf16[128,1,96]{0,2,1:T(8,128)(2,1)S(1)} %get-tuple-element.42), kind=kOutput, calls=%fused_computation.26 | convolution fusion | flops 403177472 | bytes 8437760 | tf_op jit(solution)/shard_map/cond/branch_1_fun/hqe,khe->hqk/dot_general | solution.py:72
  320.5 7.2 %fusion.28 = (bf16[8192,16]{0,1:T(8,128)(2,1)S(1)}, bf16[8192,16]{0,1:T(8,128)(2,1)S(1)}) fusion(f32[8192]{0:T(1024)S(1)} %convert_element_type.101, f32[16]{0:T(128)S(1)} %negate_power_fusion, f32[8192]{0:T(1024)S(1)} %convert_element_type.99, bf16[8192,32]{0,1:T(8,128)(2,1)S(1)} %get-tuple-element.43, f32[8192]{0:T(1024)S(1)} %convert_element_type.103, ...), kind=kLoop, calls=%fused_computation.34 | loop fusion | flops 1835008 | bytes 1179712 | tf_op jit(solution)/shard_map/convert.2
  327.6 5.8 %fusion.93 = (f32[128]{0:T(128)S(1)}, f32[128,8192]{0,1:T(8,128)}) fusion(f32[8192,128]{1,0:T(8,128)} %fusion.20, bf16[1,128,32]{1,2,0:T(8,128)(2,1)S(1)} %get-tuple-element.112, bf16[8192,16]{0,1:T(8,128)(2,1)S(1)} %get-tuple-element.121, bf16[8192,16]{0,1:T(8,128)(2,1)S(1)} %get-tuple-element.120, s32[128]{0:T(128)S(1)} %get-tuple-element.39, ...), kind=kOutput, calls=%fused_computation.110 | convolution fusion | flops 73400192 | bytes 8954880 | tf_op jit(solution)/shard_map/cond/branch_1_fun/hqr,kr->hqk/dot_general | solution.py:73
  333.5 6.3 %fusion.19 = f32[8192,128]{1,0:T(8,128)} fusion(bf16[8192,256]{1,0:T(8,128)(2,1)} %bitcast, bf16[256,128]{1,0:T(8,128)(2,1)S(1)} %get-tuple-element.68, bf16[128,1,160]{2,0,1:T(8,128)(2,1)S(1)} %copy.38), kind=kOutput, calls=%fused_computation.25 | convolution fusion | flops 806354944 | bytes 8486912 | tf_op jit(solution)/shard_map/cond/branch_1_fun/hqe,khe->hqk/dot_general | solution.py:72
  339.8 5.8 %fusion.92 = (f32[128]{0:T(128)S(1)}, f32[128,8192]{0,1:T(8,128)}) fusion(f32[8192,128]{1,0:T(8,128)} %fusion.19, bf16[1,128,32]{1,2,0:T(8,128)(2,1)S(1)} %get-tuple-element.116, bf16[8192,16]{0,1:T(8,128)(2,1)S(1)} %get-tuple-element.121, bf16[8192,16]{0,1:T(8,128)(2,1)S(1)} %get-tuple-element.120, s32[128]{0:T(128)S(1)} %get-tuple-element.39, ...), kind=kOutput, calls=%fused_computation.109 | convolution fusion | flops 73400192 | bytes 8954880 | tf_op jit(solution)/shard_map/cond/branch_1_fun/hqr,kr->hqk/dot_general | solution.py:73
  345.6 6.0 %fusion.21 = f32[1,128,128]{2,1,0:T(8,128)S(1)} fusion(bf16[8192,256]{1,0:T(8,128)(2,1)} %bitcast, bf16[256,128]{1,0:T(8,128)(2,1)S(1)} %get-tuple-element.69, f32[128,8192]{0,1:T(8,128)} %get-tuple-element.123, f32[128]{0:T(128)S(1)} %get-tuple-element.126, s32[128]{0:T(128)S(1)} %get-tuple-element.39, s32[8192]{0:T(1024)S(1)} %get-tuple-element.47), kind=kOutput, calls=%fused_computation.27 | convolution fusion | flops 810549248 | bytes 8553472 | tf_op jit(solution)/shard_map/cond/branch_1_fun/hqk,khe->hqe/dot_general | solution.py:81
  351.5 5.6 %fusion.24 = f32[1,128,64]{1,2,0:T(8,128)S(1)} fusion(f32[128,8192]{0,1:T(8,128)} %get-tuple-element.125, f32[128]{0:T(128)S(1)} %get-tuple-element.127, s32[128]{0:T(128)S(1)} %get-tuple-element.39, s32[8192]{0:T(1024)S(1)} %get-tuple-element.47, bf16[8192,256]{1,0:T(8,128)(2,1)} %bitcast, bf16[256,64]{0,1:T(8,128)(2,1)S(1)} %get-tuple-element.113), kind=kOutput, calls=%fused_computation.28 | convolution fusion | flops 407371776 | bytes 8487936 | tf_op jit(solution)/shard_map/cond/branch_1_fun/hqk,khe->hqe/dot_general | solution.py:81
  357.2 6.6 %fusion.9 = (f32[128]{0:T(128)S(1)}, f32[128]{0:T(128)S(1)}) fusion(f32[128,8192]{0,1:T(8,128)} %get-tuple-element.123, f32[128]{0:T(128)S(1)} %get-tuple-element.126, s32[128]{0:T(128)S(1)} %get-tuple-element.39, s32[8192]{0:T(1024)S(1)} %get-tuple-element.47, f32[128,8192]{0,1:T(8,128)} %get-tuple-element.125, f32[128]{0:T(128)S(1)} %get-tuple-element.127), kind=kLoop, calls=%fused_computation.17 | loop fusion | flops 7339776 | bytes 8423936 | tf_op jit(solution)/shard_map/cond/branch_1_fun/reduce_sum | solution.py:80
  364.2 1.2 fusion.45
  365.4 26.6 %all-to-all-start.1 = ((bf16[8,16,2048]{2,1,0:T(8,128)(2,1)}), bf16[8,16,2048]{2,1,0:T(8,128)(2,1)S(1)}, u32[]{:S(2)}, u32[]{:S(2)}) async-start(bf16[8,16,2048]{2,1,0:T(8,128)(2,1)} %bitcast.22), calls=%async_computation.1 | async-start | bytes 1048576 | tf_op jit(solution)/shard_map/all_to_all | solution.py:21
  391.9 9.3 %all-to-all-done.1 = bf16[8,16,2048]{2,1,0:T(8,128)(2,1)S(1)} async-done(((bf16[8,16,2048]{2,1,0:T(8,128)(2,1)}), bf16[8,16,2048]{2,1,0:T(8,128)(2,1)S(1)}, u32[]{:S(2)}, u32[]{:S(2)}) %all-to-all-start.1) | async-done | bytes 524320 | tf_op jit(solution)/shard_map/all_to_all | solution.py:21
  401.6 0.9 broadcast_in_dim.17
  402.5 4.4 all-to-all-start.2
  406.8 9.4 %all-to-all-done.2 = bf16[8,16,2048]{2,1,0:T(8,128)(2,1)S(1)} async-done(((bf16[8,16,2048]{2,1,0:T(8,128)(2,1)}), bf16[8,16,2048]{2,1,0:T(8,128)(2,1)S(1)}, u32[]{:S(2)}, u32[]{:S(2)}) %all-to-all-start.2) | async-done | bytes 524320 | tf_op jit(solution)/shard_map/all_to_all | solution.py:40
  416.2 3.2 fusion.43
  419.4 7.2 %fusion.46 = bf16[128,2048]{1,0:T(8,128)(2,1)S(1)} fusion(bf16[2048,2112]{1,0:T(8,128)(2,1)} %all-gather.2.cloned.1.call-done, bf16[128,2048]{1,0:T(8,128)(2,1)S(1)} %bitcast.68, f32[128,704]{0,1:T(8,128)S(1)} %fusion.43), kind=kOutput, calls=%fused_computation.58 | convolution fusion | flops 739000320 | bytes 7700480 | tf_op jit(solution)/shard_map/dot_general | solution.py:206
  426.7 12.7 %all_to_all.20 = bf16[8,16,2048]{2,1,0:T(8,128)(2,1)S(1)} all-to-all(bf16[8,16,2048]{2,1,0:T(8,128)(2,1)S(1)} %bitcast.69), channel_id=1, replica_groups=mesh['sp'=64,'tp'=8] {'tp'}, dimensions={0} | all-to-all | bytes 1048576 | tf_op jit(solution)/shard_map/all_to_all | solution.py:21
  439.4 0.7 fusion.66
  (52 shorter events, 1.2 us)
Async XLA Ops:
  6.5 357.6 %copy-start = (bf16[128,2048]{1,0:T(8,128)(2,1)S(1)}, bf16[128,2048]{1,0:T(8,128)(2,1)}, u32[]{:S(2)}) copy-start(bf16[128,2048]{1,0:T(8,128)(2,1)} %param.27) | copy-start | bytes 1572868
  9.9 19.8 %copy-start.5 = (bf16[32,704]{1,0:T(8,128)(2,1)S(1)}, bf16[32,704]{1,0:T(8,128)(2,1)}, u32[]{:S(2)}) copy-start(bf16[32,704]{1,0:T(8,128)(2,1)} %param.29) | copy-start | bytes 135172
  9.9 19.8 %copy-start.6 = (bf16[32,704]{1,0:T(8,128)(2,1)S(1)}, bf16[32,704]{1,0:T(8,128)(2,1)}, u32[]{:S(2)}) copy-start(bf16[32,704]{1,0:T(8,128)(2,1)} %param.30) | copy-start | bytes 135172
  9.9 19.8 %copy-start.7 = (bf16[32,704]{1,0:T(8,128)(2,1)S(1)}, bf16[32,704]{1,0:T(8,128)(2,1)}, u32[]{:S(2)}) copy-start(bf16[32,704]{1,0:T(8,128)(2,1)} %param.31) | copy-start | bytes 135172
  9.9 21.9 %copy-start.4 = (bf16[128,160]{0,1:T(8,128)(2,1)S(1)}, bf16[128,160]{0,1:T(8,128)(2,1)}, u32[]{:S(2)}) copy-start(bf16[128,160]{0,1:T(8,128)(2,1)} %param.19) | copy-start | bytes 122884
  9.9 21.9 %copy-start.9 = (bf16[128,96]{0,1:T(8,128)(2,1)S(1)}, bf16[128,96]{0,1:T(8,128)(2,1)}, u32[]{:S(2)}) copy-start(bf16[128,96]{0,1:T(8,128)(2,1)} %param.18) | copy-start | bytes 73732
  9.9 22.0 %copy-start.10 = (bf16[128,32]{0,1:T(8,128)(2,1)S(1)}, bf16[128,32]{0,1:T(8,128)(2,1)}, u32[]{:S(2)}) copy-start(bf16[128,32]{0,1:T(8,128)(2,1)} %param.21) | copy-start | bytes 24580
  9.9 304.1 %copy-start.3 = (bf16[256,128]{1,0:T(8,128)(2,1)S(1)}, bf16[256,128]{1,0:T(8,128)(2,1)}, u32[]{:S(2)}) copy-start(bf16[256,128]{1,0:T(8,128)(2,1)} %param.24) | copy-start | bytes 196612
  9.9 304.1 %copy-start.8 = (bf16[256,64]{0,1:T(8,128)(2,1)S(1)}, bf16[256,64]{0,1:T(8,128)(2,1)}, u32[]{:S(2)}) copy-start(bf16[256,64]{0,1:T(8,128)(2,1)} %param.22) | copy-start | bytes 98308
  9.9 304.1 %copy-start.12 = (bf16[256,128]{1,0:T(8,128)(2,1)S(1)}, bf16[256,128]{1,0:T(8,128)(2,1)}, u32[]{:S(2)}) copy-start(bf16[256,128]{1,0:T(8,128)(2,1)} %param.25) | copy-start | bytes 196612
  9.9 304.1 %copy-start.13 = (bf16[256,64]{0,1:T(8,128)(2,1)S(1)}, bf16[256,64]{0,1:T(8,128)(2,1)}, u32[]{:S(2)}) copy-start(bf16[256,64]{0,1:T(8,128)(2,1)} %param.23) | copy-start | bytes 98308
  9.9 304.0 %all-to-all-start = ((bf16[64,128,256]{2,1,0:T(8,128)(2,1)}), bf16[64,128,256]{2,1,0:T(8,128)(2,1)}, u32[]{:S(2)}, u32[]{:S(2)}) async-start(bf16[64,128,256]{2,1,0:T(8,128)(2,1)} %stack.2), calls=%async_computation | async-start | bytes 8388608 | tf_op jit(solution)/shard_map/all_to_all | solution.py:139
  29.6 377.2 %all-gather.2.cloned.1.call-start = ((), (), s32[]{:S(2)}) async-start(), calls=%async_computation.4 | async-start | bytes 9052160 | tf_op jit(solution)/shard_map/all_gather | solution.py:28
  314.0 49.8 %copy-start.2 = (bf16[64,2048]{1,0:T(8,128)(2,1)S(1)}, bf16[64,2048]{1,0:T(8,128)(2,1)}, u32[]{:S(2)}) copy-start(bf16[64,2048]{1,0:T(8,128)(2,1)} %param.26) | copy-start | bytes 786436
  363.8 28.1 %copy-start.11 = (bf16[2048]{0:T(1024)(128)(2,1)S(1)}, bf16[2048]{0:T(1024)(128)(2,1)}, u32[]{:S(2)}) copy-start(bf16[2048]{0:T(1024)(128)(2,1)} %param.28) | copy-start | bytes 12292
  363.8 37.5 %copy-start.1 = (bf16[16,2048]{1,0:T(8,128)(2,1)S(1)}, bf16[16,2048]{1,0:T(8,128)(2,1)}, u32[]{:S(2)}) copy-start(bf16[16,2048]{1,0:T(8,128)(2,1)} %param.17) | copy-start | bytes 196612
  365.4 35.9 %all-to-all-start.1 = ((bf16[8,16,2048]{2,1,0:T(8,128)(2,1)}), bf16[8,16,2048]{2,1,0:T(8,128)(2,1)S(1)}, u32[]{:S(2)}, u32[]{:S(2)}) async-start(bf16[8,16,2048]{2,1,0:T(8,128)(2,1)} %bitcast.22), calls=%async_computation.1 | async-start | bytes 1048576 | tf_op jit(solution)/shard_map/all_to_all | solution.py:21
  402.5 13.7 %all-to-all-start.2 = ((bf16[8,16,2048]{2,1,0:T(8,128)(2,1)}), bf16[8,16,2048]{2,1,0:T(8,128)(2,1)S(1)}, u32[]{:S(2)}, u32[]{:S(2)}) async-start(bf16[8,16,2048]{2,1,0:T(8,128)(2,1)} %broadcast_in_dim.17), calls=%async_computation.2 | async-start | bytes 1048576 | tf_op jit(solution)/shard_map/all_to_all | solution.py:40
Sparse Core Ops, SparseCore 0:
  33.4 240.0 all-gather.1
